TPU v7x, 32 devices: a whole 2x2x4 slice. The times are simulated.
32 devices in a mesh: sp: 4 (over z), fs: 4 (over y, x), tp: 2 (over core).
Axes of the slice: x: 2, y: 2, z: 4, core: 2. Of those that a mesh axis runs over, the one named last changes fastest.
Arguments:
- tokens: bfloat16 [4, 1024, 2048], P('fs', ('sp', 'tp')), may hold values from -6 to 6
- norm_gain: float32 [2048], replicated, may hold values from 0.1 to 1.9
- w_query: bfloat16 [2048, 1024], P('fs', 'tp'), may hold values from -0.125 to 0.125
- w_key: bfloat16 [2048, 1024], P('fs', 'tp'), may hold values from -0.125 to 0.125
- w_value: bfloat16 [2048, 1024], P('fs', 'tp'), may hold values from -0.125 to 0.125
- w_conv_value: bfloat16 [2048, 1024], P('fs', 'tp'), may hold values from -2 to 2
- w_conv_gate: bfloat16 [2048, 1024], P('fs', 'tp'), may hold values from -0.125 to 0.125
- key_offset: bfloat16 [1024, 16], P('sp', 'tp'), may hold values from -16 to 2
- conv_kernel: float32 [31, 1024], P(None, 'tp'), may hold values from -3 to 3
- conv_gain: float32 [1024], P('tp'), may hold values from 0.1 to 1.9
- w_attn_out: bfloat16 [1024, 2048], P('tp', 'fs'), may hold values from -1 to 1
- w_conv_out: bfloat16 [1024, 2048], P('tp', 'fs'), may hold values from -0.1875 to 0.1875
Outputs:
- mixed: bfloat16 [4, 1024, 2048], P('fs', ('sp', 'tp'))
All inputs are finite; a program needn't handle non-finite values.
Results may differ from a plain program's by a relative error of at most 0.0085.
Values may be sent and summed in bfloat16 or wider, within the bound.
A program may use at most 128 MiB of HBM per device.

v0:
```python
import functools

import jax
import jax.numpy as jnp
from jax import lax
from jax.experimental import pallas as pl
from jax.experimental.pallas import tpu as pltpu
from jax.sharding import PartitionSpec as P

HD = 64
CC = 1024
MESH = pl.DeviceIdType.MESH
F32 = jnp.float32
BF16 = jnp.bfloat16


def remote(src, dst, send, recv, **where):
    return pltpu.make_async_remote_copy(
        src_ref=src, dst_ref=dst, send_sem=send, recv_sem=recv, device_id=where, device_id_type=MESH
    )


def greet(peers):
    barrier = pltpu.get_barrier_semaphore()
    for where in peers:
        pl.semaphore_signal(barrier, inc=1, device_id=where, device_id_type=MESH)
    pl.semaphore_wait(barrier, len(peers))


def plane(fs):
    y = (fs + 2) % 4
    return fs + 1 - 2 * (fs % 2), y, y + 1 - 2 * (y % 2)


class OutGather:
    def __init__(self, source, target, sems):
        half = source.shape[0] // 2
        self.sources = [source.at[pl.ds(k * half, half)] for k in range(2)]
        self.target = target
        self.send, self.recv, self.psend, self.precv, self.local = sems
        self.fs, self.tp = lax.axis_index("fs"), lax.axis_index("tp")

    def slot(self, k, owner, group):
        rows, cols = self.sources[k].shape
        return self.target.at[
            pl.ds(pl.multiple_of((group * 2 + k) * rows, rows), rows),
            pl.ds(pl.multiple_of(owner * cols, cols), cols),
        ]

    def hop(self, src, k, owner, sem, to):
        return remote(src, self.slot(k, owner, self.tp), self.send.at[sem], self.recv.at[sem], fs=to)

    def other(self, src, k, owner, sem):
        return remote(
            src, self.slot(k, owner, self.tp), self.psend.at[sem], self.precv.at[sem], tp=1 - self.tp
        )

    def plan(self):
        fs = self.fs
        xn, yn, dg = plane(fs)
        a, c = self.sources
        self.first = [
            self.hop(a, 0, fs, 0, xn), self.hop(c, 1, fs, 1, yn),
            self.hop(c, 1, fs, 2, xn), self.hop(a, 0, fs, 3, yn),
        ]
        self.relay = [
            self.hop(self.slot(0, xn, self.tp), 0, xn, 4, yn),
            self.hop(self.slot(1, yn, self.tp), 1, yn, 5, xn),
        ]
        arrivals = [(0, 0, xn), (1, 1, yn), (2, 1, xn), (3, 0, yn), (4, 0, dg), (5, 1, dg)]
        self.got = [
            (self.hop(self.slot(k, o, self.tp), k, o, s, xn), self.other(self.slot(k, o, self.tp), k, o, s))
            for s, k, o in arrivals
        ]
        self.own = [self.other(a, 0, fs, 6), self.other(c, 1, fs, 7)]
        self.keep = [
            pltpu.make_async_copy(self.sources[k], self.slot(k, fs, self.tp), self.local.at[k]) for k in (0, 1)
        ]

    def start(self):
        self.plan()
        for copy in self.first + self.own + self.keep:
            copy.start()

    def middle(self):
        for s in range(4):
            arrived, onward = self.got[s]
            arrived.wait_recv()
            if s < 2:
                self.relay[s].start()
            onward.start()

    def finish(self):
        for s in (4, 5):
            arrived, onward = self.got[s]
            arrived.wait_recv()
            onward.start()
        for copy in self.first + self.relay:
            copy.wait_send()
        for _, onward in self.got:
            onward.wait()
        for copy in self.own:
            copy.wait()
        for copy in self.keep:
            copy.wait()


OUT_SEMS = [
    pltpu.SemaphoreType.DMA((6,)),
    pltpu.SemaphoreType.DMA((6,)),
    pltpu.SemaphoreType.DMA((8,)),
    pltpu.SemaphoreType.DMA((8,)),
    pltpu.SemaphoreType.DMA((2,)),
]


def gather_kernel(n_sp, with_out, *refs):
    tok, w_ins, off = refs[0], refs[1:6], refs[6]
    refs = refs[7:]
    if with_out:
        out_source, cgain, refs = refs[0], refs[1], refs[2:]
    tok_all, w_all, off_all = refs[:3]
    refs = refs[3:]
    if with_out:
        out_target, cgain_all, refs = refs[0], refs[1], refs[2:]
    stage, up_s, up_r, dn_s, dn_r, par_s, par_r, w_s, w_r, off_s, off_r, loc = refs[:12]
    z, fs, tp = lax.axis_index("sp"), lax.axis_index("fs"), lax.axis_index("tp")
    xn, yn, dg = plane(fs)
    rows = w_ins[0].shape[0]
    width = stage.shape[1] // 5
    half = rows // 2

    fills = [
        pltpu.make_async_copy(
            w.at[:, pl.ds(pl.multiple_of(z * width, width), width)],
            stage.at[:, pl.ds(k * width, width)],
            loc.at[k],
        )
        for k, w in enumerate(w_ins)
    ]
    for fill in fills:
        fill.start()
    keep_tok = pltpu.make_async_copy(tok, tok_all.at[z, tp], loc.at[5])
    keep_off = pltpu.make_async_copy(off, off_all.at[z], loc.at[6])
    keep_gain = pltpu.make_async_copy(cgain, cgain_all.at[tp], loc.at[8])
    keep_tok.start()
    keep_off.start()
    keep_gain.start()
    greet(
        [{"sp": (z + d) % n_sp} for d in range(1, n_sp)]
        + [{"fs": xn}, {"fs": yn}, {"tp": 1 - tp}]
    )

    def lift(src, block, dist):
        return remote(src, tok_all.at[block, tp], up_s.at[dist - 1], up_r.at[dist - 1], sp=(z + 1) % n_sp)

    def sink(src, block, dist):
        return remote(src, tok_all.at[block, tp], dn_s.at[dist - 1], dn_r.at[dist - 1], sp=(z + n_sp - 1) % n_sp)

    def across(src, block):
        return remote(src, tok_all.at[block, tp], par_s.at[block], par_r.at[block], tp=1 - tp)

    @pl.when(z < n_sp - 1)
    def _():
        lift(tok, z, 1).start()

    @pl.when(z > 0)
    def _():
        sink(tok, z, 1).start()

    across(tok, z).start()
    offs = [
        remote(off, off_all.at[z], off_s.at[d - 1], off_r.at[d - 1], sp=(z + d) % n_sp) for d in range(1, n_sp)
    ]
    gain_copy = remote(cgain, cgain_all.at[tp], refs[17].at[0], refs[17].at[1], tp=1 - tp)
    gain_copy.start()
    for copy in offs:
        copy.start()
    for fill in fills:
        fill.wait()
    keep_w = pltpu.make_async_copy(stage, w_all.at[pl.ds(pl.multiple_of(fs * rows, rows), rows)], loc.at[7])
    keep_w.start()

    def part(owner, h):
        return w_all.at[pl.ds(pl.multiple_of(owner * rows + h * half, half), half)]

    def send_w(src, owner, h, sem, to):
        return remote(src, part(owner, h), w_s.at[sem], w_r.at[sem], fs=to)

    own = [stage.at[pl.ds(h * half, half)] for h in range(2)]
    first = [
        send_w(own[0], fs, 0, 0, xn), send_w(own[1], fs, 1, 1, yn),
        send_w(own[1], fs, 1, 2, xn), send_w(own[0], fs, 0, 3, yn),
    ]
    for copy in first:
        copy.start()
    relay = [send_w(part(xn, 0), xn, 0, 4, yn), send_w(part(yn, 1), yn, 1, 5, xn)]
    if with_out:
        gather = OutGather(out_source, out_target, refs[12:17])
    arrivals = [(0, xn, 0), (1, yn, 1), (2, xn, 1), (3, yn, 0), (4, dg, 0), (5, dg, 1)]
    for s, owner, h in arrivals[:2]:
        send_w(part(owner, h), owner, h, s, xn).wait_recv()
        relay[s].start()
    if with_out:
        gather.start()

    for dist in range(1, n_sp):
        if with_out and dist == n_sp - 1:
            gather.middle()

        @pl.when(z >= dist)
        def _():
            block = (z - dist + n_sp) % n_sp
            lift(tok_all.at[block, tp], block, dist).wait_recv()
            if dist < n_sp - 1:
                @pl.when(z < n_sp - 1)
                def _():
                    lift(tok_all.at[block, tp], block, dist + 1).start()
            across(tok_all.at[block, tp], block).start()

        @pl.when(z + dist < n_sp)
        def _():
            block = (z + dist) % n_sp
            sink(tok_all.at[block, tp], block, dist).wait_recv()
            if dist < n_sp - 1:
                @pl.when(z > 0)
                def _():
                    sink(tok_all.at[block, tp], block, dist + 1).start()
            across(tok_all.at[block, tp], block).start()

    for s, owner, h in arrivals[2:]:
        send_w(part(owner, h), owner, h, s, xn).wait_recv()
    if with_out:
        gather.finish()
    for copy in first + relay:
        copy.wait_send()
    for dist in range(1, n_sp):
        @pl.when(jnp.logical_and(z < n_sp - 1, z >= dist - 1))
        def _():
            lift(tok, z, dist).wait_send()

        @pl.when(jnp.logical_and(z > 0, z + dist - 1 < n_sp))
        def _():
            sink(tok, z, dist).wait_send()

    for block in range(n_sp):
        remote(tok, tok_all.at[block, 1 - tp], par_s.at[block], par_r.at[block], tp=1 - tp).wait()
    for copy in offs:
        copy.wait()
    gain_copy.wait()
    keep_gain.wait()
    keep_tok.wait()
    keep_off.wait()
    keep_w.wait()


ANY = pl.BlockSpec(memory_space=pl.ANY)
VMEM = pl.BlockSpec(memory_space=pltpu.VMEM)


def gather_call(n_sp, n_fs, n_tp, width, tokens, w_ins, offsets, w_out, conv_gain):
    rows, features = tokens.shape
    depth = w_ins[0].shape[0]
    o_rows, o_cols = w_out.shape
    dma = pltpu.SemaphoreType.DMA
    return pl.pallas_call(
        functools.partial(gather_kernel, n_sp, True),
        out_shape=[
            jax.ShapeDtypeStruct((n_sp, n_tp, rows, features), BF16),
            jax.ShapeDtypeStruct((n_fs * depth, 5 * width), BF16),
            jax.ShapeDtypeStruct((n_sp,) + offsets.shape, F32),
            jax.ShapeDtypeStruct((n_tp * o_rows, n_fs * o_cols), BF16),
            jax.ShapeDtypeStruct((n_tp,) + conv_gain.shape, F32),
        ],
        in_specs=[ANY] * 9,
        out_specs=[ANY] * 5,
        scratch_shapes=[
            pltpu.VMEM((depth, 5 * width), BF16),
            dma((n_sp - 1,)), dma((n_sp - 1,)), dma((n_sp - 1,)), dma((n_sp - 1,)),
            dma((n_sp,)), dma((n_sp,)),
            dma((6,)), dma((6,)),
            dma((n_sp - 1,)), dma((n_sp - 1,)),
            dma((9,)),
        ] + OUT_SEMS + [dma((2,))],
        compiler_params=pltpu.CompilerParams(collective_id=0, has_side_effects=True),
        name="gather_inputs",
    )(tokens, *w_ins, offsets, w_out, conv_gain)


def compute_body(n_sp, n_tp, width, heads, taps, blk, *refs):
    tok_hbm, gain, w_hbm, off, ck, cgain, wa_hbm, wc_own, mixed = refs[:9]
    attn_out, conv_out, mean_out, proj, gated, wa, wc, x_all, mean_all, send, recv, loc, wa_sem, tok, w, tok_sem = refs[9:25]
    length, n_rows = tok.shape[0], mean_out.shape[2]
    gather = OutGather(wc_own, wc, refs[25:])
    z, tp, fs = lax.axis_index("sp"), lax.axis_index("tp"), lax.axis_index("fs")
    xn, yn, _ = plane(fs)
    me, place, n = z * n_tp + tp, tp * n_sp + z, n_sp * n_tp
    fetch = pltpu.make_async_copy(wa_hbm, wa, wa_sem.at[0])
    load_w = pltpu.make_async_copy(w_hbm, w, wa_sem.at[1])

    def load(i):
        at = pl.ds(pl.multiple_of(i * 128, 128), 128)
        return pltpu.make_async_copy(tok_hbm.at[at], tok.at[at], tok_sem.at[i])

    load_w.start()
    for i in range(length // 128):
        load(i).start()
    fetch.start()
    peers = [(me + d) % n for d in range(1, n)]
    greet([{"sp": p // n_tp, "tp": p % n_tp} for p in peers] + [{"fs": xn}, {"fs": yn}])
    gather.start()

    def pair(k, dest, slot):
        at = pl.ds(pl.multiple_of(dest * n_rows, n_rows), n_rows)
        if k == 2:
            return mean_out.at[dest], mean_all.at[slot]
        there = pl.ds(pl.multiple_of((k * n + slot) * width, width), width)
        return (attn_out, conv_out)[k].at[at], x_all.at[:, there]

    def ship(k, sp, core):
        src, dst = pair(k, sp * n_tp + core, place)
        mine = jnp.logical_and(z == sp, tp == core)

        @pl.when(mine)
        def _():
            pltpu.make_async_copy(src, dst, loc.at[k]).start()

        @pl.when(jnp.logical_not(mine))
        def _():
            remote(src, dst, send.at[k, sp * n_tp + core], recv.at[k, place], sp=sp, tp=core).start()

    def project(i, _):
        at = pl.ds(pl.multiple_of(i * 128, 128), 128)
        load(i).wait()
        x = tok[at, :].astype(F32)
        normed = (x * lax.rsqrt(jnp.mean(x * x, axis=1, keepdims=True) + 1e-06) * gain[...]).astype(BF16)
        out = jnp.dot(normed, w[...], preferred_element_type=F32).astype(BF16)
        proj[at, :] = out[:, : 3 * width]
        value = out[:, 3 * width : 4 * width].astype(F32)
        gate = out[:, 4 * width :].astype(F32)
        gated[pl.ds(pl.multiple_of(i * 128 + 32, 32), 128), :] = (value * jax.nn.sigmoid(gate)).astype(BF16).astype(F32)
        return 0

    gated[pl.ds(0, 32), :] = jnp.zeros((32, width), F32)
    load_w.wait()
    lax.fori_loop(0, length // 128, project, 0)

    ones = jnp.full((8, width), 1.0 / width, F32)

    def convolve(i, _):
        base = pl.multiple_of(i * n_rows, n_rows)
        window = gated[pl.ds(base, n_rows + 32), :]
        total = jnp.zeros((n_rows, width), F32)
        for tap in range(taps):
            lo = 32 - (taps - 1) + tap
            total = total + ck[tap : tap + 1, pl.ds(pl.multiple_of(z * width, width), width)] * window[lo : lo + n_rows]
        local = jnp.mean(total, axis=1, keepdims=True)
        conv_out[pl.ds(base, n_rows), :] = (total - local).astype(BF16)
        mean_out[i] = lax.dot_general(
            ones, total, (((1,), (1,)), ((), ())), precision=lax.Precision.HIGHEST, preferred_element_type=F32
        )
        return 0

    lax.fori_loop(0, length // n_rows, convolve, 0)

    row = lax.broadcasted_iota(jnp.int32, (blk, blk), 0)
    col = lax.broadcasted_iota(jnp.int32, (blk, blk), 1)
    allowed = col < row
    after = jnp.where(row >= col, 1.0, 0.0).astype(BF16)
    lane = lax.broadcasted_iota(jnp.int32, (blk, width), 1)

    def attend(i):
        q_at = pl.ds(i * blk, blk)
        mine = [jnp.logical_and(lane >= h * HD, lane < (h + 1) * HD) for h in range(heads)]
        q_all = proj[q_at, :width].astype(F32) * HD ** (-0.5)
        qs = [jnp.where(m, q_all, 0.0).astype(BF16) for m in mine]

        def pieces(j, state, diagonal):
            k_at = pl.ds(pl.multiple_of(j * blk, blk), blk)
            k = proj[k_at, width : 2 * width]
            v = proj[k_at, 2 * width : 3 * width]
            result = []
            for h, (carry, total) in enumerate(state):
                s = lax.dot_general(qs[h], k, (((1,), (1,)), ((), ())), preferred_element_type=F32)
                s = s + off[j, pl.ds(z * heads + h, 1), :]
                keep = jnp.minimum(-s, 0.0) - jnp.log(1.0 + jnp.exp(-jnp.abs(s)))
                if diagonal:
                    keep = jnp.where(allowed, keep, 0.0)
                high = keep.astype(BF16)
                low = (keep - high.astype(F32)).astype(BF16)
                suffix = jnp.dot(high, after, preferred_element_type=F32)
                suffix = suffix + jnp.dot(low, after, preferred_element_type=F32)
                weights = jnp.exp(s + suffix + carry)
                if diagonal:
                    weights = jnp.where(allowed, weights, 0.0)
                total = total + jnp.dot(weights.astype(BF16), v, preferred_element_type=F32)
                result.append((carry + suffix[:, :1], total))
            return tuple(result)

        state = tuple((jnp.zeros((blk, 1), F32), jnp.zeros((blk, width), F32)) for _ in range(heads))
        state = pieces(i, state, True)
        if i:
            state = lax.fori_loop(0, i, lambda t, c: pieces(i - 1 - t, c, False), state)
        merged = state[0][1]
        for h in range(1, heads):
            merged = jnp.where(mine[h], state[h][1], merged)
        attn_out[q_at, :] = merged.astype(BF16)

    for step, i in enumerate(reversed(range(n_sp))):
        attend(i)
        if step == 0:
            for sp in range(n_sp):
                for core in range(n_tp):
                    ship(1, sp, core)
                    ship(2, sp, core)
        else:
            for core in range(n_tp):
                ship(0, i + 1, core)
        if step == (n_sp - 1) // 2:
            gather.middle()
    gather.finish()
    for core in range(n_tp):
        ship(0, 0, core)
    fetch.wait()

    def arrive(k):
        src, dst = pair(k, me, place)
        pltpu.make_async_copy(src, dst, loc.at[k]).wait()
        for d in range(1, n):
            source = (me - d + n) % n
            slot = (source % n_tp) * n_sp + source // n_tp
            src, dst = pair(k, me, slot)
            remote(src, dst, send.at[k, me], recv.at[k, slot], tp=1 - tp).wait_recv()

    arrive(2)
    arrive(1)
    square = (lax.broadcasted_iota(jnp.int32, (n_rows, n_rows), 0)
              == lax.broadcasted_iota(jnp.int32, (n_rows, n_rows), 1)).astype(F32)
    local = [
        lax.dot_general(square, mean_all[g], (((1,), (1,)), ((), ())),
                        precision=lax.Precision.HIGHEST, preferred_element_type=F32)[:, :1]
        for g in range(n)
    ]
    mean = sum(local) / n
    base = n * width
    centred = [
        x_all[:, base + g * width : base + (g + 1) * width].astype(F32) + (local[g] - mean) for g in range(n)
    ]
    shift = sum(jnp.sum(c, axis=1, keepdims=True) for c in centred) / base
    centred = [c - shift for c in centred]
    spread = sum(jnp.sum(c * c, axis=1, keepdims=True) for c in centred) / base
    scale = lax.rsqrt(spread + 1e-06)
    hidden = []
    for g, c in enumerate(centred):
        y = c * scale * cgain[:, g * width : (g + 1) * width]
        hidden.append((y * jax.nn.sigmoid(y)).astype(BF16))
    hidden = jnp.concatenate(hidden, axis=1)
    arrive(0)
    chunk = wc_own.shape[1]

    def output(c, _):
        at = pl.ds(pl.multiple_of(c * chunk, chunk), chunk)
        total = jnp.dot(x_all[:, :base], wa[:, at], preferred_element_type=F32)
        total = total + jnp.dot(hidden, wc[:, at], preferred_element_type=F32)
        mixed[:, at] = total.astype(BF16)
        return 0

    lax.fori_loop(0, wc.shape[1] // chunk, output, 0)
    for d in range(1, n):
        p = (me + d) % n
        for k in range(3):
            src, dst = pair(k, p, place)
            remote(src, dst, send.at[k, p], recv.at[k, place], tp=1 - tp).wait_send()


def compute_call(n_sp, n_tp, width, heads, blk, tok, gain, w, off, ck, cgain, wa, w_out):
    length = tok.shape[0]
    n = n_sp * n_tp
    rows = length // n
    dma = pltpu.SemaphoreType.DMA
    return pl.pallas_call(
        functools.partial(compute_body, n_sp, n_tp, width, heads, ck.shape[0], blk),
        out_shape=jax.ShapeDtypeStruct((rows, wa.shape[1]), BF16),
        in_specs=[ANY, VMEM, ANY] + [VMEM] * 3 + [ANY] * 2,
        out_specs=VMEM,
        scratch_shapes=[
            pltpu.VMEM((length, width), BF16),
            pltpu.VMEM((length, width), BF16),
            pltpu.VMEM((n, 8, rows), F32),
            pltpu.VMEM((length, 3 * width), BF16),
            pltpu.VMEM((length + 32, width), F32),
            pltpu.VMEM(wa.shape, BF16),
            pltpu.VMEM(wa.shape, BF16),
            pltpu.VMEM((rows, 2 * n * width), BF16),
            pltpu.VMEM((n, 8, rows), F32),
            dma((3, n)), dma((3, n)), dma((3,)), dma((2,)),
            pltpu.VMEM(tok.shape, BF16),
            pltpu.VMEM(w.shape, BF16),
            dma((length // 128,)),
        ] + OUT_SEMS,
        compiler_params=pltpu.CompilerParams(collective_id=1, has_side_effects=True),
        name="branches",
    )(tok, gain, w, off, ck, cgain, wa, w_out)


def spread_shards(
    tokens,
    norm_gain,
    w_query,
    w_key,
    w_value,
    w_conv_value,
    w_conv_gate,
    key_offset,
    conv_kernel,
    conv_gain,
    w_attn_out,
    w_conv_out,
):
    n_sp, n_fs, n_tp = (lax.axis_size(a) for a in ("sp", "fs", "tp"))
    width = w_query.shape[1] // n_sp
    heads = width // HD
    offsets = jnp.transpose(key_offset.astype(F32))
    tok_all, w_all, off_all, wa, cgain = gather_call(
        n_sp, n_fs, n_tp, width, tokens[0],
        (w_query, w_key, w_value, w_conv_value, w_conv_gate), offsets, w_attn_out, conv_gain[None],
    )
    tok_all = tok_all.reshape(-1, tokens.shape[2])
    mixed = compute_call(
        n_sp, n_tp, width, heads, key_offset.shape[0], tok_all, norm_gain[None], w_all, off_all, conv_kernel,
        cgain.reshape(1, -1), wa, w_conv_out,
    )
    return mixed[None]


def shifted(block, axis, distance):
    devices = range(lax.axis_size(axis))
    route = [(i - distance, i) for i in devices if i - distance in devices]
    return lax.ppermute(block, axis, route)


def piece_terms(queries, key_rows, value_rows, offsets, carry_log, allowed):
    head_size = queries.shape[2]
    logits = jnp.einsum(
        "qhd,khd->hqk", queries, key_rows, preferred_element_type=jnp.float32
    ) * head_size ** (-0.5)
    logits = logits + jnp.transpose(offsets.astype(jnp.float32))[:, None, :]
    log_keep = jax.nn.log_sigmoid(-logits)
    if allowed is not None:
        log_keep = jnp.where(allowed[None], log_keep, 0.0)
    between = lax.cumsum(log_keep, axis=2, reverse=True) - log_keep
    weights = jnp.exp(jax.nn.log_sigmoid(logits) + between + carry_log[:, :, None])
    if allowed is not None:
        weights = jnp.where(allowed[None], weights, 0.0)
    result = jnp.einsum(
        "hqk,khd->qhd", weights.astype(jnp.bfloat16), value_rows, preferred_element_type=jnp.float32
    )
    return (result, carry_log + jnp.sum(log_keep, axis=2))


def shards(
    tokens,
    norm_gain,
    w_query,
    w_key,
    w_value,
    w_conv_value,
    w_conv_gate,
    key_offset,
    conv_kernel,
    conv_gain,
    w_attn_out,
    w_conv_out,
):
    gathered = (
        lax.all_gather(w_query, "fs", axis=0, tiled=True),
        lax.all_gather(w_key, "fs", axis=0, tiled=True),
        lax.all_gather(w_value, "fs", axis=0, tiled=True),
        lax.all_gather(w_conv_value, "fs", axis=0, tiled=True),
        lax.all_gather(w_conv_gate, "fs", axis=0, tiled=True),
    )
    floats = lax.all_gather(tokens[0], "tp", axis=0, tiled=True).astype(jnp.float32)
    normed = (
        floats * lax.rsqrt(jnp.mean(floats * floats, axis=1, keepdims=True) + 1e-06) * norm_gain
    ).astype(jnp.bfloat16)
    projected = jnp.concatenate(
        [
            jnp.dot(normed, weight, preferred_element_type=jnp.float32).astype(jnp.bfloat16)
            for weight in gathered
        ],
        axis=1,
    )
    head_cols = w_query.shape[1]
    channels = w_conv_value.shape[1]
    block_len = projected.shape[0]
    local_heads = head_cols // HD
    queries = projected[:, :head_cols].reshape(block_len, local_heads, HD)
    key_flat = projected[:, head_cols : 2 * head_cols]
    value_flat = projected[:, 2 * head_cols : 3 * head_cols]
    conv_value = projected[:, 3 * head_cols : 3 * head_cols + channels]
    conv_gate = projected[:, 3 * head_cols + channels :]
    position = lax.axis_index("sp")
    positions = jnp.arange(block_len, dtype=jnp.int32)
    causal = positions[None, :] < positions[:, None]
    start_log = jnp.zeros((local_heads, block_len), jnp.float32)
    totals, carry_log = piece_terms(
        queries,
        key_flat.reshape(block_len, local_heads, HD),
        value_flat.reshape(block_len, local_heads, HD),
        key_offset,
        start_log,
        causal,
    )

    def visit(hop_count, carried):
        running, running_log, moving = carried
        moving = shifted((moving[0], moving[1], moving[2]), "sp", 1)
        result, next_log = piece_terms(
            queries,
            moving[0].reshape(block_len, local_heads, HD),
            moving[1].reshape(block_len, local_heads, HD),
            moving[2],
            running_log,
            None,
        )
        active = position >= hop_count
        running = jnp.where(active, running + result, running)
        running_log = jnp.where(active, next_log, running_log)
        return (running, running_log, moving)

    totals, carry_log, leftover = lax.fori_loop(
        1, lax.axis_size("sp"), visit, (totals, carry_log, (key_flat, value_flat, key_offset))
    )
    attn_heads = totals.reshape(block_len, head_cols).astype(jnp.bfloat16)
    gated_input = (
        conv_value.astype(jnp.float32) * jax.nn.sigmoid(conv_gate.astype(jnp.float32))
    ).astype(jnp.bfloat16)
    kernel_len = conv_kernel.shape[0]
    edge_rows = shifted(gated_input[block_len - (kernel_len - 1) :], "sp", 1)
    extended = jnp.concatenate([edge_rows, gated_input], axis=0).astype(jnp.float32)
    conv_sum = jnp.zeros((block_len, channels), jnp.float32)
    for tap_index in range(kernel_len):
        conv_sum = conv_sum + conv_kernel[tap_index] * extended[tap_index : tap_index + block_len]
    channel_total = lax.psum(jnp.sum(conv_sum, axis=1), "tp")
    centred = conv_sum - (channel_total / CC)[:, None]
    spread = lax.psum(jnp.sum(centred * centred, axis=1), "tp") / CC
    conv_hidden = jax.nn.silu(centred * lax.rsqrt(spread + 1e-06)[:, None] * conv_gain).astype(
        jnp.bfloat16
    )
    attn_weight, conv_weight = (
        lax.all_gather(w_attn_out, "fs", axis=1, tiled=True),
        lax.all_gather(w_conv_out, "fs", axis=1, tiled=True),
    )
    partial_value = jnp.dot(attn_heads, attn_weight, preferred_element_type=jnp.float32)
    partial_value = partial_value + jnp.dot(
        conv_hidden, conv_weight, preferred_element_type=jnp.float32
    )
    mixed = lax.psum_scatter(
        lax.optimization_barrier(partial_value.astype(jnp.bfloat16))
        .astype(jnp.float32)
        .astype(jnp.bfloat16),
        "tp",
        scatter_dimension=0,
        tiled=True,
    )
    return mixed[None]


def solution(mesh):
    placed = (
        P("fs", ("sp", "tp"), None),
        P(),
        P("fs", "tp"),
        P("fs", "tp"),
        P("fs", "tp"),
        P("fs", "tp"),
        P("fs", "tp"),
        P("sp", "tp"),
        P(None, "tp"),
        P("tp"),
        P("tp", "fs"),
        P("tp", "fs"),
    )

    def fits(tokens, norm_gain, w_query, *rest):
        n_sp, n_fs, n_tp = mesh.shape["sp"], mesh.shape["fs"], mesh.shape["tp"]
        cols = w_query.shape[1] // n_tp
        return n_fs == 4 and n_tp == 2 and n_sp > 1 and rest[5].shape[0] <= 33 and cols % (128 * n_sp) == 0 and rest[2].shape[1] == w_query.shape[1] and (
            tokens.shape[1] % (128 * n_sp * n_tp) == 0
        )

    def program(*args):
        body = spread_shards if fits(*args) else shards
        return mapped(body)(*args)

    def mapped(body):
        return jax.shard_map(
            body, mesh=mesh, in_specs=placed, out_specs=P("fs", ("sp", "tp"), None), check_vma=False
        )

    return program
```

profile of v0, /device:TPU:0, one launch (start us, length us, event | category | flops | bytes accessed | tf_op | source)
XLA Modules:
  0.0 90.1 jit_solution(4512423742090721357)
XLA Ops:
  0.0 1.3 %convert_bitcast_fusion.refs_6_ = f32[8,256]{1,0:T(8,128)} fusion(bf16[256,8]{0,1:T(8,128)(2,1)} %param.19), kind=kLoop, calls=%fused_computation | loop fusion | flops 2048 | bytes 12288 | tf_op jit(solution)/shard_map/transpose | solution.py:523
  1.3 47.7 %gather_inputs.1 = (bf16[4,2,128,2048]{3,2,1,0:T(8,128)(2,1)}, bf16[2048,640]{1,0:T(8,128)(2,1)}, f32[4,8,256]{2,1,0:T(8,128)}, bf16[1024,2048]{1,0:T(8,128)(2,1)}, f32[2,1,512]{2,1,0:T(1,128)}) custom-call(bf16[128,2048]{1,0:T(8,128)(2,1)} %bitcast.10, bf16[512,512]{1,0:T(8,128)(2,1)} %refs_1_.1, bf16[512,512]{1,0:T(8,128)(2,1)} %refs_2_.1, ...), custom_call_target="tpu_custom_call" | custom-call | tf_op jit(solution)/shard_map/gather_inputs/pallas_call | solution.py:266
  49.0 39.2 %branches.1 = bf16[128,2048]{1,0:T(8,128)(2,1)} custom-call(bf16[1024,2048]{1,0:T(8,128)(2,1)} %bitcast.8, f32[1,2048]{1,0:T(1,128)} %bitcast.11, bf16[2048,640]{1,0:T(8,128)(2,1)} %get-tuple-element.11.refs_2_, f32[4,8,256]{2,1,0:T(8,128)} %get-tuple-element.12.refs_3_, f32[31,512]{1,0:T(8,128)} %refs_4_.3, f32[1,1024]{1,0:T(1,128)} %bitcast.12, ...), custom_call_target="tpu_custom_call" | custom-call | tf_op jit(solution)/shard_map/branches/pallas_call | solution.py:481
  88.2 1.9 %copy.14 = bf16[1,128,2048]{2,1,0:T(8,128)(2,1)} copy(bf16[1,128,2048]{2,1,0:T(8,128)(2,1)} %bitcast.9) | data formatting | bytes 1048576
where the time goes:
time: 90.3 us; the launch traced here: 90.1 us
  Pallas kernels  86.9 us (96%)
  local copies, waits for them, and re-layouts  1.88 us (2%)
  other arithmetic  1.29 us (1%)
    pallas_call x1, Pallas kernels, gather_call(): pl.pallas_call(functools.partial(gather_kernel, n_sp, True), out_shape=[j...  47.7 us
    pallas_call x1, Pallas kernels, compute_call(): pl.pallas_call(functools.partial(compute_body, n_sp, n_tp, width, heads,...  39.2 us
    unnamed x1, local copies, waits for them, and re-layouts  1.88 us

commit v1 on v0

v1 whole, which is shorter than its diff:
```python
import functools

import jax
import jax.numpy as jnp
from jax import lax
from jax.experimental import pallas as pl
from jax.experimental.pallas import tpu as pltpu
from jax.sharding import PartitionSpec as P

HD = 64
CC = 1024
MESH = pl.DeviceIdType.MESH
F32 = jnp.float32
BF16 = jnp.bfloat16


def remote(src, dst, send, recv, **where):
    return pltpu.make_async_remote_copy(
        src_ref=src, dst_ref=dst, send_sem=send, recv_sem=recv, device_id=where, device_id_type=MESH
    )


def greet(peers):
    barrier = pltpu.get_barrier_semaphore()
    for where in peers:
        pl.semaphore_signal(barrier, inc=1, device_id=where, device_id_type=MESH)
    pl.semaphore_wait(barrier, len(peers))


def plane(fs):
    y = (fs + 2) % 4
    return fs + 1 - 2 * (fs % 2), y, y + 1 - 2 * (y % 2)


ANY = pl.BlockSpec(memory_space=pl.ANY)


def aligned(start, size):
    return pl.ds(pl.multiple_of(start, size), size)


def layer_body(n_sp, n_tp, width, heads, taps, blk, *refs):
    tok_in, gain_in, w_ins, off_in, ck_in, cgain_in, wa_in, wc_in = refs[0], refs[1], refs[2:7], *refs[7:12]
    own_out, got_out = refs[12:14]
    tok, w, wout, off_raw, off, ck, gain, cgain = refs[14:22]
    queries, keys, values, gated, carry, running = refs[22:28]
    attn_out, conv_out, stat_out, x_all, stat_all, hidden, part = refs[28:35]
    ld, up_s, up_r, dn_s, dn_r, par_s, par_r, w_s, w_r, off_s, off_r = refs[35:46]
    o_s, o_r, x_s, x_r, st_s, st_r, part_s, part_r, keep_s = refs[46:]
    rows = tok_in.shape[0]
    sub = rows // 2
    depth = w_ins[0].shape[0]
    half = depth // 2
    o_rows, o_cols = wa_in.shape
    quarter = o_rows // 2
    z, fs, tp = lax.axis_index("sp"), lax.axis_index("fs"), lax.axis_index("tp")
    xn, yn, dg = plane(fs)
    n = n_sp * n_tp
    me = z * n_tp + tp

    own_rows = aligned((z * n_tp + tp) * rows, rows)
    loads = [pltpu.make_async_copy(tok_in, tok.at[own_rows], ld.at[0])]
    loads += [
        pltpu.make_async_copy(
            ref.at[:, aligned(z * width, width)],
            w.at[aligned(fs * depth, depth), pl.ds(k * width, width)],
            ld.at[1 + k],
        )
        for k, ref in enumerate(w_ins)
    ]
    loads += [
        pltpu.make_async_copy(wa_in, wout.at[fs, pl.ds(0, o_rows)], ld.at[6]),
        pltpu.make_async_copy(wc_in, wout.at[fs, pl.ds(o_rows, o_rows)], ld.at[7]),
        pltpu.make_async_copy(off_in, off_raw.at[z], ld.at[8]),
        pltpu.make_async_copy(ck_in.at[:, aligned(z * width, width)], ck, ld.at[9]),
        pltpu.make_async_copy(gain_in, gain, ld.at[10]),
        pltpu.make_async_copy(cgain_in, cgain, ld.at[11]),
    ]
    for copy in loads:
        copy.start()
    greet(
        [{"sp": (me + d) % n // n_tp, "tp": (me + d) % n % n_tp} for d in range(1, n)]
        + [{"fs": xn}, {"fs": yn}]
    )

    def piece_rows(block, core, p):
        return tok.at[aligned((block * n_tp + core) * rows + p * sub, sub)]

    def lift(block, dist, p):
        ref = piece_rows(block, tp, p)
        return remote(ref, ref, up_s.at[dist - 1, p], up_r.at[dist - 1, p], sp=(z + 1) % n_sp)

    def sink(block, dist, p):
        ref = piece_rows(block, tp, p)
        return remote(ref, ref, dn_s.at[dist - 1, p], dn_r.at[dist - 1, p], sp=(z + n_sp - 1) % n_sp)

    def across(block, p):
        ref = piece_rows(block, tp, p)
        return remote(ref, ref, par_s.at[block, p], par_r.at[block, p], tp=1 - tp)

    def from_partner(block, p):
        ref = piece_rows(block, 1 - tp, p)
        return remote(ref, ref, par_s.at[block, p], par_r.at[block, p], tp=1 - tp)

    def w_part(owner, h):
        return w.at[aligned(owner * depth + h * half, half)]

    def send_w(owner, h, sem, to):
        return remote(w_part(owner, h), w_part(owner, h), w_s.at[sem], w_r.at[sem], fs=to)

    def send_o(owner, k, sem, to):
        ref = wout.at[owner, pl.ds(k * quarter, quarter)]
        return remote(ref, ref, o_s.at[sem], o_r.at[sem], fs=to)

    loads[0].wait()
    for p in range(2):
        @pl.when(z < n_sp - 1)
        def _():
            lift(z, 1, p).start()

        @pl.when(z > 0)
        def _():
            sink(z, 1, p).start()

    for k in range(5):
        loads[1 + k].wait()
    w_first = [send_w(fs, 0, 0, xn), send_w(fs, 1, 1, yn), send_w(fs, 1, 2, xn), send_w(fs, 0, 3, yn)]
    for copy in w_first:
        copy.start()
    for p in range(2):
        across(z, p).start()
    loads[8].wait()
    offs = [
        remote(off_raw.at[z], off_raw.at[z], off_s.at[d - 1], off_r.at[d - 1], sp=(z + d) % n_sp)
        for d in range(1, n_sp)
    ]
    for copy in offs:
        copy.start()
    w_relay = [send_w(xn, 0, 4, yn), send_w(yn, 1, 5, xn)]
    w_here = [(0, xn, 0), (1, yn, 1), (2, xn, 1), (3, yn, 0), (4, dg, 0), (5, dg, 1)]
    o_first = []
    for a, b in ((0, 2), (1, 3), (2, 0), (3, 1)):
        o_first += [send_o(fs, a, a, xn), send_o(fs, b, 4 + b, yn)]
    o_relay = [send_o(xn, 0, 8, yn), send_o(yn, 2, 10, xn), send_o(xn, 1, 9, yn), send_o(yn, 3, 11, xn)]

    def token_hop(dist, p):
        @pl.when(z >= dist)
        def _():
            block = (z - dist + n_sp) % n_sp
            lift(block, dist, p).wait_recv()
            if dist < n_sp - 1:
                @pl.when(z < n_sp - 1)
                def _():
                    lift(block, dist + 1, p).start()
            across(block, p).start()

        @pl.when(z + dist < n_sp)
        def _():
            block = (z + dist) % n_sp
            sink(block, dist, p).wait_recv()
            if dist < n_sp - 1:
                @pl.when(z > 0)
                def _():
                    sink(block, dist + 1, p).start()
            across(block, p).start()

    def relay_w():
        for s, owner, h in w_here[:2]:
            send_w(owner, h, s, xn).wait_recv()
            w_relay[s].start()
        for copy in loads[6:8]:
            copy.wait()
        for copy in o_first:
            copy.start()

    gated[pl.ds(0, 32), :] = jnp.zeros((32, width), F32)
    for dist in range(1, n_sp - 1):
        token_hop(dist, 0)
        if dist == 1:
            relay_w()
        token_hop(dist, 1)
    if n_sp == 2:
        relay_w()
    for copy in loads[9:]:
        copy.wait()
    for s, owner, h in w_here[2:]:
        send_w(owner, h, s, xn).wait_recv()
    for copy in offs:
        copy.wait()
    off[...] = off_raw[...].astype(F32)

    lane = lax.broadcasted_iota(jnp.int32, (rows, width), 1)

    def project(tile, _):
        at = aligned(tile * rows, rows)
        x = tok[at, :].astype(F32)
        normed = (x * lax.rsqrt(jnp.mean(x * x, axis=1, keepdims=True) + 1e-06) * gain[...]).astype(BF16)
        out = jnp.dot(normed, w[...], preferred_element_type=F32).astype(BF16)
        q = out[:, :width].astype(F32) * HD ** (-0.5)
        for h in range(heads):
            mine = jnp.logical_and(lane >= h * HD, lane < (h + 1) * HD)
            queries[h, at, :] = jnp.where(mine, q, 0.0).astype(BF16)
        keys[at, :] = out[:, width : 2 * width]
        values[at, :] = out[:, 2 * width : 3 * width]
        value = out[:, 3 * width : 4 * width].astype(F32)
        gate = out[:, 4 * width :].astype(F32)
        gated[pl.ds(pl.multiple_of(tile * rows + 32, 32), rows), :] = (
            (value * jax.nn.sigmoid(gate)).astype(BF16).astype(F32)
        )
        return 0

    ones = jnp.full((8, width), 1.0 / width, F32)
    top = lax.broadcasted_iota(jnp.int32, (8, rows), 0) == 0

    def average(x):
        return lax.dot_general(
            ones, x, (((1,), (1,)), ((), ())), precision=lax.Precision.HIGHEST, preferred_element_type=F32
        )

    def convolve(tile, _):
        base = pl.multiple_of(tile * rows, rows)
        window = gated[pl.ds(base, rows + 32), :]
        total = jnp.zeros((rows, width), F32)
        for tap in range(taps):
            lo = 32 - (taps - 1) + tap
            total = total + ck[tap : tap + 1, :] * window[lo : lo + rows]
        local = total - jnp.mean(total, axis=1, keepdims=True)
        conv_out[pl.ds(base, rows), :] = local.astype(BF16)
        stat_out[tile] = jnp.where(top, average(total), average(local * local))
        return 0

    def block_rows(i):
        return aligned(i * blk, blk)

    def ship(k, source, block):
        at = source.at[block_rows(block)]

        @pl.when(block == z)
        def _():
            x_all[k * n_sp + z] = at[...]

        @pl.when(block != z)
        def _():
            remote(at, x_all.at[k * n_sp + z], x_s.at[k, block], x_r.at[k, z], sp=block).start()

    tiles = blk // rows

    def ship_stat(block):
        at = stat_out.at[pl.ds(block * tiles, tiles)]

        @pl.when(block == z)
        def _():
            stat_all[z] = at[...]

        @pl.when(block != z)
        def _():
            remote(at, stat_all.at[z], st_s.at[0, block], st_r.at[z], sp=block).start()

        remote(at, stat_all.at[n_sp + z], st_s.at[1, block], st_r.at[n_sp + z], sp=block, tp=1 - tp).start()

    row = lax.broadcasted_iota(jnp.int32, (blk, blk), 0)
    col = lax.broadcasted_iota(jnp.int32, (blk, blk), 1)
    wide = lax.broadcasted_iota(jnp.int32, (blk, width), 1)

    def attend(i, j, diagonal):
        k = keys[block_rows(j), :]
        v = values[block_rows(j), :]
        after = jnp.where(row >= col, 1.0, 0.0).astype(BF16)
        for h in range(heads):
            q = queries[h, block_rows(i), :]
            s = lax.dot_general(q, k, (((1,), (1,)), ((), ())), preferred_element_type=F32)
            s = s + off[j, pl.ds(z * heads + h, 1), :]
            keep = jnp.minimum(-s, 0.0) - jnp.log(1.0 + jnp.exp(-jnp.abs(s)))
            if diagonal:
                keep = jnp.where(col < row, keep, 0.0)
            high = keep.astype(BF16)
            low = (keep - high.astype(F32)).astype(BF16)
            suffix = jnp.dot(high, after, preferred_element_type=F32)
            suffix = suffix + jnp.dot(low, after, preferred_element_type=F32)
            if diagonal:
                weights = jnp.where(col < row, jnp.exp(s + suffix), 0.0)
                carry[i, h] = suffix[:, :1]
                running[i, h] = jnp.dot(weights.astype(BF16), v, preferred_element_type=F32)
            else:
                before = carry[i, h]
                weights = jnp.exp(s + suffix + before)
                carry[i, h] = before + suffix[:, :1]
                running[i, h] += jnp.dot(weights.astype(BF16), v, preferred_element_type=F32)

        @pl.when(j == 0)
        def _():
            merged = running[i, 0]
            for h in range(1, heads):
                merged = jnp.where(wide >= h * HD, running[i, h], merged)
            attn_out[block_rows(i), :] = merged.astype(BF16)
            ship(0, attn_out, i)

    pairs = jnp.minimum(z, n_sp - 1 - z)

    def step(s, _):
        dist = (s + 1) // 2
        inner = jnp.where(s % 2 == 1, z - dist, z + dist)
        outer = jnp.where(z == pairs, s, n_sp - 1 - s)
        block = jnp.where(s <= 2 * pairs, inner, outer)
        rising = block > z

        @pl.when(jnp.logical_and(s == n_sp - 1, pairs == 0))
        def _():
            for p in range(2):
                token_hop(n_sp - 1, p)

        for p in range(2):
            from_partner(block, p).wait_recv()
        lax.fori_loop(block * n_tp, block * n_tp + n_tp, project, 0)

        def conv_block(u, _):
            target = jnp.where(rising, block, jnp.where(jnp.logical_and(u == 0, s > 0), block + 1, 0))
            lax.fori_loop(target * tiles, target * tiles + tiles, convolve, 0)
            ship(1, conv_out, target)
            ship_stat(target)
            return 0

        falling_count = jnp.where(s > 0, 1, 0) + jnp.where(block == 0, 1, 0)
        lax.fori_loop(0, jnp.where(rising, 1, falling_count), conv_block, 0)
        attend(block, block, True)

        def further(t, _):
            attend(jnp.where(rising, block, block + t), jnp.where(rising, block - t, block), False)
            return 0

        lax.fori_loop(1, s + 1, further, 0)
        return 0

    lax.fori_loop(0, n_sp, step, 0)
    for k in (0, 1):
        send_o(xn, k, k, xn).wait_recv()
        send_o(yn, 2 + k, 6 + k, xn).wait_recv()
    for copy in o_relay:
        copy.start()

    others = [(z + d) % n_sp for d in range(1, n_sp)]

    def stat_from(slot):
        return remote(stat_all.at[slot], stat_all.at[slot], st_s.at[0, z], st_r.at[slot], tp=1 - tp)

    def x_from(k, source):
        ref = x_all.at[k * n_sp + source]
        return remote(ref, ref, x_s.at[k, z], x_r.at[k, source], tp=1 - tp)

    for source in others:
        stat_from(source).wait_recv()
    for source in range(n_sp):
        stat_from(n_sp + source).wait_recv()
    for source in others:
        x_from(1, source).wait_recv()
    square = (lax.broadcasted_iota(jnp.int32, (rows, rows), 0)
              == lax.broadcasted_iota(jnp.int32, (rows, rows), 1)).astype(F32)
    kind = lax.broadcasted_iota(jnp.int32, (rows, n * 8), 1) % 8
    for t in range(tiles):
        flat = stat_all[:, t].reshape(n * 8, rows)
        stats = lax.dot_general(
            square, flat, (((1,), (1,)), ((), ())), precision=lax.Precision.HIGHEST, preferred_element_type=F32
        )
        mean = jnp.sum(jnp.where(kind == 0, stats, 0.0), axis=1, keepdims=True) / n
        off_mean = stats - mean
        spread = jnp.where(kind == 0, off_mean * off_mean, jnp.where(kind == 1, stats, 0.0))
        scale = lax.rsqrt(jnp.sum(spread, axis=1, keepdims=True) / n + 1e-06)
        at = pl.ds(t * rows, rows)
        for g in range(n_sp):
            x = x_all[n_sp + g, at, :].astype(F32) + off_mean[:, 8 * g : 8 * g + 1]
            y = x * scale * cgain[:, g * width : (g + 1) * width]
            hidden[at, (n_sp + g) * width : (n_sp + g + 1) * width] = (y * jax.nn.sigmoid(y)).astype(BF16)
    for source in others:
        x_from(0, source).wait_recv()
    for g in range(n_sp):
        hidden[:, g * width : (g + 1) * width] = x_all[g]

    sent = []
    for index, owner in enumerate((fs, xn, yn, dg)):
        if owner is xn:
            for k in (2, 3):
                send_o(xn, k, k, xn).wait_recv()
        elif owner is yn:
            for k in (0, 1):
                send_o(yn, k, 4 + k, xn).wait_recv()
        elif owner is dg:
            for k in range(4):
                send_o(dg, k, 8 + k, xn).wait_recv()
        part[index] = jnp.dot(hidden[...], wout[owner], preferred_element_type=F32).astype(BF16)
        cols = aligned(owner * o_cols, o_cols)
        keep = pltpu.make_async_copy(
            part.at[index, aligned(tp * rows, rows)], own_out.at[:, cols], keep_s.at[index]
        )
        give = remote(
            part.at[index, aligned((1 - tp) * rows, rows)], got_out.at[:, cols],
            part_s.at[index], part_r.at[index], tp=1 - tp,
        )
        give.start()
        keep.start()
        sent += [keep, give]

    for copy in w_first + w_relay + o_first + o_relay:
        copy.wait_send()
    for p in range(2):
        for dist in range(1, n_sp):
            @pl.when(jnp.logical_and(z < n_sp - 1, z >= dist - 1))
            def _():
                lift(z, dist, p).wait_send()

            @pl.when(jnp.logical_and(z > 0, z + dist - 1 < n_sp))
            def _():
                sink(z, dist, p).wait_send()

        for block in range(n_sp):
            across(block, p).wait_send()
    for block in others:
        for k in range(2):
            remote(x_all.at[k], x_all.at[k], x_s.at[k, block], x_r.at[k, z], tp=1 - tp).wait_send()
        remote(stat_all.at[z], stat_all.at[z], st_s.at[0, block], st_r.at[z], tp=1 - tp).wait_send()
    for block in range(n_sp):
        remote(stat_all.at[z], stat_all.at[z], st_s.at[1, block], st_r.at[z], tp=1 - tp).wait_send()
    for copy in sent:
        copy.wait()


def layer_call(n_sp, n_fs, n_tp, width, heads, blk, tokens, gain, w_ins, off, ck, cgain, wa, wc):
    rows, features = tokens.shape
    depth = w_ins[0].shape[0]
    o_rows, o_cols = wa.shape
    length, n = rows * n_sp * n_tp, n_sp * n_tp
    tiles = blk // rows
    dma = pltpu.SemaphoreType.DMA
    vmem = pltpu.VMEM
    result = jax.ShapeDtypeStruct((rows, n_fs * o_cols), BF16)
    return pl.pallas_call(
        functools.partial(layer_body, n_sp, n_tp, width, heads, ck.shape[0], blk),
        out_shape=[result, result],
        in_specs=[ANY] * 12,
        out_specs=[ANY] * 2,
        scratch_shapes=[
            vmem((length, features), BF16),
            vmem((n_fs * depth, 5 * width), BF16),
            vmem((n_fs, 2 * o_rows, o_cols), BF16),
            vmem((n_sp,) + off.shape, BF16),
            vmem((n_sp,) + off.shape, F32),
            vmem((ck.shape[0], width), F32),
            vmem(gain.shape, F32),
            vmem(cgain.shape, F32),
            vmem((heads, length, width), BF16),
            vmem((length, width), BF16),
            vmem((length, width), BF16),
            vmem((length + 32, width), F32),
            vmem((n_sp, heads, blk, 1), F32),
            vmem((n_sp, heads, blk, width), F32),
            vmem((length, width), BF16),
            vmem((length, width), BF16),
            vmem((length // rows, 8, rows), F32),
            vmem((2 * n_sp, blk, width), BF16),
            vmem((n, tiles, 8, rows), F32),
            vmem((blk, 2 * n_sp * width), BF16),
            vmem((n_fs, blk, o_cols), BF16),
            dma((12,)),
            dma((n_sp - 1, 2)), dma((n_sp - 1, 2)), dma((n_sp - 1, 2)), dma((n_sp - 1, 2)),
            dma((n_sp, 2)), dma((n_sp, 2)),
            dma((6,)), dma((6,)),
            dma((n_sp - 1,)), dma((n_sp - 1,)),
            dma((12,)), dma((12,)),
            dma((2, n_sp)), dma((2, n_sp)),
            dma((2, n_sp)), dma((n,)),
            dma((n_fs,)), dma((n_fs,)), dma((n_fs,)),
        ],
        compiler_params=pltpu.CompilerParams(collective_id=0, has_side_effects=True),
        name="layer",
    )(tokens, gain, *w_ins, off, ck, cgain, wa, wc)


def spread_shards(
    tokens,
    norm_gain,
    w_query,
    w_key,
    w_value,
    w_conv_value,
    w_conv_gate,
    key_offset,
    conv_kernel,
    conv_gain,
    w_attn_out,
    w_conv_out,
):
    n_sp, n_fs, n_tp = (lax.axis_size(a) for a in ("sp", "fs", "tp"))
    width = w_query.shape[1] // n_sp
    own, got = layer_call(
        n_sp, n_fs, n_tp, width, width // HD, key_offset.shape[0], tokens[0], norm_gain[None],
        (w_query, w_key, w_value, w_conv_value, w_conv_gate), jnp.transpose(key_offset),
        conv_kernel, conv_gain[None], w_attn_out, w_conv_out,
    )
    return (own.astype(F32) + got.astype(F32)).astype(BF16)[None]


def shifted(block, axis, distance):
    devices = range(lax.axis_size(axis))
    route = [(i - distance, i) for i in devices if i - distance in devices]
    return lax.ppermute(block, axis, route)


def piece_terms(queries, key_rows, value_rows, offsets, carry_log, allowed):
    head_size = queries.shape[2]
    logits = jnp.einsum(
        "qhd,khd->hqk", queries, key_rows, preferred_element_type=jnp.float32
    ) * head_size ** (-0.5)
    logits = logits + jnp.transpose(offsets.astype(jnp.float32))[:, None, :]
    log_keep = jax.nn.log_sigmoid(-logits)
    if allowed is not None:
        log_keep = jnp.where(allowed[None], log_keep, 0.0)
    between = lax.cumsum(log_keep, axis=2, reverse=True) - log_keep
    weights = jnp.exp(jax.nn.log_sigmoid(logits) + between + carry_log[:, :, None])
    if allowed is not None:
        weights = jnp.where(allowed[None], weights, 0.0)
    result = jnp.einsum(
        "hqk,khd->qhd", weights.astype(jnp.bfloat16), value_rows, preferred_element_type=jnp.float32
    )
    return (result, carry_log + jnp.sum(log_keep, axis=2))


def shards(
    tokens,
    norm_gain,
    w_query,
    w_key,
    w_value,
    w_conv_value,
    w_conv_gate,
    key_offset,
    conv_kernel,
    conv_gain,
    w_attn_out,
    w_conv_out,
):
    gathered = (
        lax.all_gather(w_query, "fs", axis=0, tiled=True),
        lax.all_gather(w_key, "fs", axis=0, tiled=True),
        lax.all_gather(w_value, "fs", axis=0, tiled=True),
        lax.all_gather(w_conv_value, "fs", axis=0, tiled=True),
        lax.all_gather(w_conv_gate, "fs", axis=0, tiled=True),
    )
    floats = lax.all_gather(tokens[0], "tp", axis=0, tiled=True).astype(jnp.float32)
    normed = (
        floats * lax.rsqrt(jnp.mean(floats * floats, axis=1, keepdims=True) + 1e-06) * norm_gain
    ).astype(jnp.bfloat16)
    projected = jnp.concatenate(
        [
            jnp.dot(normed, weight, preferred_element_type=jnp.float32).astype(jnp.bfloat16)
            for weight in gathered
        ],
        axis=1,
    )
    head_cols = w_query.shape[1]
    channels = w_conv_value.shape[1]
    block_len = projected.shape[0]
    local_heads = head_cols // HD
    queries = projected[:, :head_cols].reshape(block_len, local_heads, HD)
    key_flat = projected[:, head_cols : 2 * head_cols]
    value_flat = projected[:, 2 * head_cols : 3 * head_cols]
    conv_value = projected[:, 3 * head_cols : 3 * head_cols + channels]
    conv_gate = projected[:, 3 * head_cols + channels :]
    position = lax.axis_index("sp")
    positions = jnp.arange(block_len, dtype=jnp.int32)
    causal = positions[None, :] < positions[:, None]
    start_log = jnp.zeros((local_heads, block_len), jnp.float32)
    totals, carry_log = piece_terms(
        queries,
        key_flat.reshape(block_len, local_heads, HD),
        value_flat.reshape(block_len, local_heads, HD),
        key_offset,
        start_log,
        causal,
    )

    def visit(hop_count, carried):
        running, running_log, moving = carried
        moving = shifted((moving[0], moving[1], moving[2]), "sp", 1)
        result, next_log = piece_terms(
            queries,
            moving[0].reshape(block_len, local_heads, HD),
            moving[1].reshape(block_len, local_heads, HD),
            moving[2],
            running_log,
            None,
        )
        active = position >= hop_count
        running = jnp.where(active, running + result, running)
        running_log = jnp.where(active, next_log, running_log)
        return (running, running_log, moving)

    totals, carry_log, leftover = lax.fori_loop(
        1, lax.axis_size("sp"), visit, (totals, carry_log, (key_flat, value_flat, key_offset))
    )
    attn_heads = totals.reshape(block_len, head_cols).astype(jnp.bfloat16)
    gated_input = (
        conv_value.astype(jnp.float32) * jax.nn.sigmoid(conv_gate.astype(jnp.float32))
    ).astype(jnp.bfloat16)
    kernel_len = conv_kernel.shape[0]
    edge_rows = shifted(gated_input[block_len - (kernel_len - 1) :], "sp", 1)
    extended = jnp.concatenate([edge_rows, gated_input], axis=0).astype(jnp.float32)
    conv_sum = jnp.zeros((block_len, channels), jnp.float32)
    for tap_index in range(kernel_len):
        conv_sum = conv_sum + conv_kernel[tap_index] * extended[tap_index : tap_index + block_len]
    channel_total = lax.psum(jnp.sum(conv_sum, axis=1), "tp")
    centred = conv_sum - (channel_total / CC)[:, None]
    spread = lax.psum(jnp.sum(centred * centred, axis=1), "tp") / CC
    conv_hidden = jax.nn.silu(centred * lax.rsqrt(spread + 1e-06)[:, None] * conv_gain).astype(
        jnp.bfloat16
    )
    attn_weight, conv_weight = (
        lax.all_gather(w_attn_out, "fs", axis=1, tiled=True),
        lax.all_gather(w_conv_out, "fs", axis=1, tiled=True),
    )
    partial_value = jnp.dot(attn_heads, attn_weight, preferred_element_type=jnp.float32)
    partial_value = partial_value + jnp.dot(
        conv_hidden, conv_weight, preferred_element_type=jnp.float32
    )
    mixed = lax.psum_scatter(
        lax.optimization_barrier(partial_value.astype(jnp.bfloat16))
        .astype(jnp.float32)
        .astype(jnp.bfloat16),
        "tp",
        scatter_dimension=0,
        tiled=True,
    )
    return mixed[None]


def solution(mesh):
    placed = (
        P("fs", ("sp", "tp"), None),
        P(),
        P("fs", "tp"),
        P("fs", "tp"),
        P("fs", "tp"),
        P("fs", "tp"),
        P("fs", "tp"),
        P("sp", "tp"),
        P(None, "tp"),
        P("tp"),
        P("tp", "fs"),
        P("tp", "fs"),
    )

    def fits(tokens, norm_gain, w_query, *rest):
        n_sp, n_fs, n_tp = mesh.shape["sp"], mesh.shape["fs"], mesh.shape["tp"]
        cols = w_query.shape[1] // n_tp
        return n_fs == 4 and n_tp == 2 and n_sp > 1 and rest[5].shape[0] <= 33 and cols % (128 * n_sp) == 0 and rest[2].shape[1] == w_query.shape[1] and (
            tokens.shape[1] % (128 * n_sp * n_tp) == 0
        )

    def program(*args):
        body = spread_shards if fits(*args) else shards
        return mapped(body)(*args)

    def mapped(body):
        return jax.shard_map(
            body, mesh=mesh, in_specs=placed, out_specs=P("fs", ("sp", "tp"), None), check_vma=False
        )

    return program
```

time: 90.3 us -> 71.8 us (0.80)
  Pallas kernels: 86.9 us -> 69.5 us
  local copies, waits for them, and re-layouts: 1.88 us -> 0 us
    pallas_call x2 -> x1, Pallas kernels: 86.9 us -> 69.5 us  [layer_call(): pl.pallas_call(functools.partial(layer_body, n_sp, n_tp, width, heads, ck...]
    broadcast_in_dim x0 -> x1, other arithmetic: none -> 2.12 us  [spread_shards(): return (own.astype(F32) + got.astype(F32)).astype(BF16)[None]]
    unnamed x1 -> x0, local copies, waits for them, and re-layouts: 1.88 us -> none
    transpose x1 -> x0, other arithmetic: 1.29 us -> none  [spread_shards(): offsets = jnp.transpose(key_offset.astype(F32))]
where the time goes in v1:
time: 71.8 us; the launch traced here: 71.6 us
  Pallas kernels  69.5 us (97%)
  other arithmetic  2.12 us (3%)
    pallas_call x1, Pallas kernels, layer_call(): pl.pallas_call(functools.partial(layer_body, n_sp, n_tp, width, heads, ck...  69.5 us
    broadcast_in_dim x1, other arithmetic, spread_shards(): return (own.astype(F32) + got.astype(F32)).astype(BF16)[None]  2.12 us

profile of v1, /device:TPU:0, one launch (start us, length us, event | category | flops | bytes accessed | tf_op | source)
XLA Modules:
  0.0 71.6 jit_solution(11286667251933047680)
XLA Ops:
  0.0 69.5 %layer.1 = (bf16[128,2048]{1,0:T(8,128)(2,1)}, bf16[128,2048]{1,0:T(8,128)(2,1)}) custom-call(bf16[128,2048]{1,0:T(8,128)(2,1)} %bitcast.6, f32[1,2048]{1,0:T(1,128)} %bitcast.7, bf16[512,512]{1,0:T(8,128)(2,1)} %refs_2_.1, bf16[512,512]{1,0:T(8,128)(2,1)} %refs_3_.1, bf16[512,512]{1,0:T(8,128)(2,1)} %refs_4_.1, bf16[512,512]{1,0:T(8,128)(2,1)} %refs_5_.1, ...), custom_call_target="tpu_custom_call" | custom-call | tf_op jit(solution)/shard_map/layer/pallas_call | solution.py:435
  69.5 2.1 %fusion = bf16[1,128,2048]{2,1,0:T(8,128)(2,1)} fusion(bf16[128,2048]{1,0:T(8,128)(2,1)} %get-tuple-element.8, bf16[128,2048]{1,0:T(8,128)(2,1)} %get-tuple-element.7), kind=kLoop, calls=%fused_computation.1 | loop fusion | flops 1048576 | bytes 1572864 | tf_op jit(solution)/shard_map/broadcast_in_dim | solution.py:498

commit v2 on v1

--- a/solution.py
+++ b/solution.py
@@ -219,11 +219,9 @@
 
     def convolve(tile, _):
         base = pl.multiple_of(tile * rows, rows)
-        window = gated[pl.ds(base, rows + 32), :]
         total = jnp.zeros((rows, width), F32)
         for tap in range(taps):
-            lo = 32 - (taps - 1) + tap
-            total = total + ck[tap : tap + 1, :] * window[lo : lo + rows]
+            total = total + ck[tap : tap + 1, :] * gated[pl.ds(base + (33 - taps + tap), rows), :]
         local = total - jnp.mean(total, axis=1, keepdims=True)
         conv_out[pl.ds(base, rows), :] = local.astype(BF16)
         stat_out[tile] = jnp.where(top, average(total), average(local * local))
@@ -273,10 +271,7 @@
             keep = jnp.minimum(-s, 0.0) - jnp.log(1.0 + jnp.exp(-jnp.abs(s)))
             if diagonal:
                 keep = jnp.where(col < row, keep, 0.0)
-            high = keep.astype(BF16)
-            low = (keep - high.astype(F32)).astype(BF16)
-            suffix = jnp.dot(high, after, preferred_element_type=F32)
-            suffix = suffix + jnp.dot(low, after, preferred_element_type=F32)
+            suffix = jnp.dot(keep.astype(BF16), after, preferred_element_type=F32)
             if diagonal:
                 weights = jnp.where(col < row, jnp.exp(s + suffix), 0.0)
                 carry[i, h] = suffix[:, :1]
@@ -304,6 +299,14 @@
         block = jnp.where(s <= 2 * pairs, inner, outer)
         rising = block > z
 
+        @pl.when(s == n_sp - 1)
+        def _():
+            for k in (0, 1):
+                send_o(xn, k, k, xn).wait_recv()
+                send_o(yn, 2 + k, 6 + k, xn).wait_recv()
+            for copy in o_relay:
+                copy.start()
+
         @pl.when(jnp.logical_and(s == n_sp - 1, pairs == 0))
         def _():
             for p in range(2):
@@ -313,9 +316,11 @@
             from_partner(block, p).wait_recv()
         lax.fori_loop(block * n_tp, block * n_tp + n_tp, project, 0)
 
+        lax.fori_loop(block * tiles + 1, block * tiles + tiles, convolve, 0)
+
         def conv_block(u, _):
             target = jnp.where(rising, block, jnp.where(jnp.logical_and(u == 0, s > 0), block + 1, 0))
-            lax.fori_loop(target * tiles, target * tiles + tiles, convolve, 0)
+            convolve(target * tiles, 0)
             ship(1, conv_out, target)
             ship_stat(target)
             return 0
@@ -332,11 +337,6 @@
         return 0
 
     lax.fori_loop(0, n_sp, step, 0)
-    for k in (0, 1):
-        send_o(xn, k, k, xn).wait_recv()
-        send_o(yn, 2 + k, 6 + k, xn).wait_recv()
-    for copy in o_relay:
-        copy.start()
 
     others = [(z + d) % n_sp for d in range(1, n_sp)]
 

time: 71.8 us -> 67.4 us (0.939)
  Pallas kernels: 69.5 us -> 65.2 us
    pallas_call x1, Pallas kernels: 69.5 us -> 65.2 us  [layer_call(): pl.pallas_call(functools.partial(layer_body, n_sp, n_tp, width, heads, ck...]
where the time goes in v2:
time: 67.4 us; the launch traced here: 67.3 us
  Pallas kernels  65.2 us (97%)
  other arithmetic  2.12 us (3%)
    pallas_call x1, Pallas kernels, layer_call(): pl.pallas_call(functools.partial(layer_body, n_sp, n_tp, width, heads, ck...  65.2 us
    broadcast_in_dim x1, other arithmetic, spread_shards(): return (own.astype(F32) + got.astype(F32)).astype(BF16)[None]  2.12 us

profile of v2, /device:TPU:0, one launch (start us, length us, event | category | flops | bytes accessed | tf_op | source)
XLA Modules:
  0.0 67.3 jit_solution(1572802522159210746)
XLA Ops:
  0.0 65.2 %layer.1 = (bf16[128,2048]{1,0:T(8,128)(2,1)}, bf16[128,2048]{1,0:T(8,128)(2,1)}) custom-call(bf16[128,2048]{1,0:T(8,128)(2,1)} %bitcast.6, f32[1,2048]{1,0:T(1,128)} %bitcast.7, bf16[512,512]{1,0:T(8,128)(2,1)} %refs_2_.1, bf16[512,512]{1,0:T(8,128)(2,1)} %refs_3_.1, bf16[512,512]{1,0:T(8,128)(2,1)} %refs_4_.1, bf16[512,512]{1,0:T(8,128)(2,1)} %refs_5_.1, ...), custom_call_target="tpu_custom_call" | custom-call | tf_op jit(solution)/shard_map/layer/pallas_call | solution.py:435
  65.2 2.1 %fusion = bf16[1,128,2048]{2,1,0:T(8,128)(2,1)} fusion(bf16[128,2048]{1,0:T(8,128)(2,1)} %get-tuple-element.8, bf16[128,2048]{1,0:T(8,128)(2,1)} %get-tuple-element.7), kind=kLoop, calls=%fused_computation.1 | loop fusion | flops 1048576 | bytes 1572864 | tf_op jit(solution)/shard_map/broadcast_in_dim | solution.py:498
